TPU v7x, 128 devices: a whole 4x4x4 slice. The times are simulated.
128 devices in a mesh: ra: 16 (over z, y), cb: 8 (over x, core).
Axes of the slice: x: 4, y: 4, z: 4, core: 2. Of those that a mesh axis runs over, the one named last changes fastest.
Arguments:
- tokens: bfloat16 [256, 3072], P(None, 'ra'), may hold values from -8 to 8, as said below
- first_gain: float32 [3072], P('ra'), may hold values from 0.1 to 1.9
- first_gate: float32 [3072, 8192], P('ra', 'cb'), may hold values from -0.109375 to 0.109375
- first_up: float32 [3072, 8192], P('ra', 'cb'), may hold values from -0.109375 to 0.109375
- first_down: float32 [8192, 3072], P('cb', 'ra'), may hold values from -0.0625 to 0.0625
- first_gate_scale: float32 [8192], P('cb'), may hold values from 0.5 to 2
- first_up_scale: float32 [8192], P('cb'), may hold values from 0.5 to 2
- first_down_scale: float32 [3072], P('ra'), may hold values from 0.5 to 2
- second_gain: float32 [3072], P('ra'), may hold values from 0.1 to 1.9
- second_gate: float32 [3072, 8192], P('ra', 'cb'), may hold values from -0.109375 to 0.109375
- second_up: float32 [3072, 8192], P('ra', 'cb'), may hold values from -0.109375 to 0.109375
- second_down: float32 [8192, 3072], P('cb', 'ra'), may hold values from -0.0625 to 0.0625
- second_gate_scale: float32 [8192], P('cb'), may hold values from 0.5 to 2
- second_up_scale: float32 [8192], P('cb'), may hold values from 0.5 to 2
- second_down_scale: float32 [3072], P('ra'), may hold values from 0.5 to 2
Outputs:
- mixed: bfloat16 [256, 3072], P(None, 'ra')
Inputs may be any that keep to these rules, and one draw needn't show every extreme that they name: The features come in groups of 64 with different magnitudes, and tokens differ in magnitude.
All inputs are finite; a program needn't handle non-finite values.
Results may differ from a plain program's by a relative error of at most 0.0093.
Values may be sent and summed in bfloat16 or wider, within the bound.
No kernel may reach another device: no remote copies, remote signals or barrier semaphores. Data moves between devices by JAX's collectives and lax.ppermute only.
A program may use at most 64 MiB of HBM per device.

v0:
```python
import jax
import jax.numpy as jnp
from jax import lax
from jax.sharding import PartitionSpec as P

D = 3072


def split_up(shard, dim, peers):
    before, after = (shard.shape[:dim], shard.shape[dim + 1 :])
    return jnp.moveaxis(shard.reshape(*before, peers, -1, *after), dim, 0)


def sum_at_owner(shard, axis, dim):
    peers = lax.axis_size(axis)
    tiles = lax.all_to_all(split_up(shard, dim, peers), axis, 0, 0, tiled=True)
    return jnp.sum(tiles, axis=0)


def side_by_side(arrays, axis, dim, along):
    columns = [a.reshape(*a.shape[:along], -1) for a in arrays]
    both = jnp.concatenate(columns, axis=along)
    result, at, finished = (sum_at_owner(both, axis, dim), 0, [])
    for a, column in zip(arrays, columns):
        slab = result[..., at : at + column.shape[along]]
        finished.append(slab.reshape(*slab.shape[:along], *a.shape[along:]))
        at += column.shape[along]
    return tuple(finished)


def from_everyone(shard, axis):
    peers = lax.axis_size(axis)
    return lax.all_to_all(
        jnp.broadcast_to(shard[None], (peers, *shard.shape)), axis, 0, 0, tiled=True
    )


def in_order(tiles, dim):
    tiles = jnp.moveaxis(tiles, 0, dim)
    shape = tiles.shape
    return tiles.reshape(*shape[:dim], shape[dim] * shape[dim + 1], *shape[dim + 2 :])


def gathered_copies(shard, axis, dim):
    tiles = from_everyone(shard, axis)
    return in_order(tiles, dim)


def of_everyone(shard, axis):
    everything = from_everyone(shard, axis)
    return jnp.sum(everything, axis=0)


def half_step(stream_in, gain, w_gate, w_up, w_down, gate_scale, up_scale, down_scale):
    stream = stream_in.astype(jnp.float32)
    squares = jnp.sum(stream * stream, axis=1)
    shaped = (stream * gain[None, :]).astype(jnp.bfloat16)
    gate_part = jnp.dot(shaped, w_gate.astype(jnp.bfloat16), preferred_element_type=jnp.float32)
    up_part = jnp.dot(shaped, w_up.astype(jnp.bfloat16), preferred_element_type=jnp.float32)
    squares_here, gate_sum, up_sum = side_by_side((squares, gate_part, up_part), "ra", 0, 1)
    inverse = lax.rsqrt(squares_here / D + 1e-06)[:, None]
    gate_full = inverse * gate_scale[None, :] * gate_sum
    up_full = inverse * up_scale[None, :] * up_sum
    hidden_share = (jax.nn.silu(gate_full) * up_full).astype(jnp.bfloat16)
    hidden = gathered_copies(hidden_share, "ra", 0)
    down_part = jnp.dot(hidden, w_down.astype(jnp.bfloat16), preferred_element_type=jnp.float32)
    down_sum = of_everyone(down_part, "cb")
    return (stream + 0.5 * down_scale[None, :] * down_sum).astype(jnp.bfloat16)


def body(
    tokens,
    first_gain,
    first_gate,
    first_up,
    first_down,
    first_gate_scale,
    first_up_scale,
    first_down_scale,
    second_gain,
    second_gate,
    second_up,
    second_down,
    second_gate_scale,
    second_up_scale,
    second_down_scale,
):
    middle = half_step(
        tokens,
        first_gain,
        first_gate,
        first_up,
        first_down,
        first_gate_scale,
        first_up_scale,
        first_down_scale,
    )
    return half_step(
        middle,
        second_gain,
        second_gate,
        second_up,
        second_down,
        second_gate_scale,
        second_up_scale,
        second_down_scale,
    )


def solution(mesh):
    return jax.shard_map(
        body,
        mesh=mesh,
        in_specs=(
            P(None, "ra"),
            P("ra"),
            P("ra", "cb"),
            P("ra", "cb"),
            P("cb", "ra"),
            P("cb"),
            P("cb"),
            P("ra"),
            P("ra"),
            P("ra", "cb"),
            P("ra", "cb"),
            P("cb", "ra"),
            P("cb"),
            P("cb"),
            P("ra"),
        ),
        out_specs=P(None, "ra"),
        check_vma=False,
    )
```

profile of v0, /device:TPU:1, one launch (start us, length us, event | category | flops | bytes accessed | tf_op | source)
XLA Modules:
  0.0 172.5 jit_solution(13957684336240065165)
XLA Ops:
  0.0 0.0 copy-start.1
  0.0 1.0 fusion.12
  1.0 1.6 fusion.10
  2.6 0.0 copy-done.1
  2.6 2.3 %fusion.8 = f32[256,1024]{1,0:T(8,128)} fusion(f32[192,1024]{1,0:T(8,128)S(1)} %copy-done.1, bf16[256,192]{0,1:T(8,128)(2,1)} %param.15, f32[192]{0:T(256)} %param.16), kind=kOutput, calls=%fused_computation.8 | convolution fusion | flops 101007360 | bytes 1934080 | tf_op jit(solution)/shard_map/dot_general | solution.py:59
  4.9 0.2 concatenate.28
  5.1 2.8 %concatenate.23 = f32[16,16,2049]{2,1,0:T(8,128)S(1)} concatenate(f32[16,16,1]{2,1,0:T(8,128)S(1)} %concatenate.28, f32[16,16,1024]{2,1,0:T(8,128)S(1)} %bitcast.10, f32[16,16,1024]{2,1,0:T(8,128)} %bitcast.11), dimensions={2} | concatenate | bytes 4196352 | tf_op jit(solution)/shard_map/concatenate | solution.py:22
  7.9 37.2 %all_to_all.30 = f32[16,16,2049]{2,1,0:T(8,128)} all-to-all(f32[16,16,2049]{2,1,0:T(8,128)S(1)} %concatenate.23), channel_id=1, replica_groups=mesh['ra'=16,'cb'=8] {'ra'}, dimensions={0} | all-to-all | bytes 4196352 | tf_op jit(solution)/shard_map/all_to_all | solution.py:16
  45.1 0.0 copy-start.7
  45.1 0.0 copy-start.8
  45.1 0.0 copy-start.4
  45.1 1.8 %reduce_sum.55 = f32[16,2049]{1,0:T(8,128)S(1)} reduce(f32[16,16,2049]{2,1,0:T(8,128)} %all_to_all.30, f32[]{:T(128)} %constant.10.clone.1), dimensions={0}, to_apply=%region_1.0 | reduce | flops 491760 | bytes 2229316 | tf_op jit(solution)/shard_map/reduce_sum | solution.py:17
  47.0 0.1 fusion.31
  47.1 0.0 copy-done.7
  47.1 0.0 copy-done.8
  47.1 0.1 fusion.21
  47.2 0.1 broadcast_in_dim.8
  47.3 12.8 %all_to_all.31 = bf16[16,16,1024]{2,1,0:T(8,128)(2,1)S(1)} all-to-all(bf16[16,16,1024]{2,1,0:T(8,128)(2,1)S(1)} %broadcast_in_dim.8), channel_id=1, replica_groups=mesh['ra'=16,'cb'=8] {'ra'}, dimensions={0} | all-to-all | bytes 1048576 | tf_op jit(solution)/shard_map/all_to_all | solution.py:33
  60.1 0.0 copy-done.4
  60.1 0.3 fusion.6
  60.4 0.0 copy-start.11
  60.4 1.3 broadcast_in_dim.9
  61.7 0.0 copy-start
  61.7 0.0 copy-start.2
  61.7 0.0 copy-start.6
  61.7 7.2 %all-to-all-start.2 = ((f32[8,256,192]{1,2,0:T(8,128)}), f32[8,256,192]{1,2,0:T(8,128)S(1)}, u32[]{:S(2)}, u32[]{:S(2)}) async-start(f32[8,256,192]{1,2,0:T(8,128)} %broadcast_in_dim.9), calls=%async_computation.2 | async-start | bytes 3145728 | tf_op jit(solution)/shard_map/all_to_all | solution.py:33
  68.9 0.0 copy-done.11
  68.9 0.0 copy-start.3
  68.9 20.6 %all-to-all-done.2 = f32[8,256,192]{1,2,0:T(8,128)S(1)} async-done(((f32[8,256,192]{1,2,0:T(8,128)}), f32[8,256,192]{1,2,0:T(8,128)S(1)}, u32[]{:S(2)}, u32[]{:S(2)}) %all-to-all-start.2) | async-done | bytes 1572896 | tf_op jit(solution)/shard_map/all_to_all | solution.py:33
  89.5 0.8 reduce_sum.56
  90.3 0.0 copy-done
  90.3 1.0 fusion.15
  91.3 0.0 copy-done.2
  91.3 0.0 copy-done.6
  91.4 0.4 fusion.4
  91.7 0.0 copy-done.3
  91.8 1.4 fusion.2
  93.1 0.2 concatenate.29
  93.4 2.8 %concatenate.27 = f32[16,16,2049]{2,1,0:T(8,128)S(1)} concatenate(f32[16,16,1]{2,1,0:T(8,128)S(1)} %concatenate.29, f32[16,16,1024]{2,1,0:T(8,128)S(1)} %bitcast.8, f32[16,16,1024]{2,1,0:T(8,128)} %bitcast.9), dimensions={2} | concatenate | bytes 4196352 | tf_op jit(solution)/shard_map/concatenate | solution.py:22
  96.2 32.0 %all_to_all.32 = f32[16,16,2049]{2,1,0:T(8,128)} all-to-all(f32[16,16,2049]{2,1,0:T(8,128)S(1)} %concatenate.27), channel_id=1, replica_groups=mesh['ra'=16,'cb'=8] {'ra'}, dimensions={0} | all-to-all | bytes 4196352 | tf_op jit(solution)/shard_map/all_to_all | solution.py:16
  128.2 0.0 copy-start.9
  128.2 0.0 copy-start.10
  128.2 0.0 copy-start.5
  128.2 1.8 %reduce_sum.58 = f32[16,2049]{1,0:T(8,128)S(1)} reduce(f32[16,16,2049]{2,1,0:T(8,128)} %all_to_all.32, f32[]{:T(128)} %constant.10.clone.1), dimensions={0}, to_apply=%region_4.5 | reduce | flops 491760 | bytes 2229316 | tf_op jit(solution)/shard_map/reduce_sum | solution.py:17
  130.0 0.1 fusion.28
  130.1 0.0 copy-done.9
  130.1 0.0 copy-done.10
  130.1 0.1 fusion.19
  130.2 0.1 broadcast_in_dim.10
  130.3 12.7 %all_to_all.33 = bf16[16,16,1024]{2,1,0:T(8,128)(2,1)S(1)} all-to-all(bf16[16,16,1024]{2,1,0:T(8,128)(2,1)S(1)} %broadcast_in_dim.10), channel_id=1, replica_groups=mesh['ra'=16,'cb'=8] {'ra'}, dimensions={0} | all-to-all | bytes 1048576 | tf_op jit(solution)/shard_map/all_to_all | solution.py:33
  143.0 0.0 copy-done.5
  143.0 0.3 fusion
  143.3 0.0 copy-start.12
  143.3 1.3 broadcast_in_dim.11
  144.6 6.4 %all-to-all-start.5 = ((f32[8,256,192]{1,2,0:T(8,128)}), f32[8,256,192]{1,2,0:T(8,128)S(1)}, u32[]{:S(2)}, u32[]{:S(2)}) async-start(f32[8,256,192]{1,2,0:T(8,128)} %broadcast_in_dim.11), calls=%async_computation.5 | async-start | bytes 3145728 | tf_op jit(solution)/shard_map/all_to_all | solution.py:33
  151.0 0.0 copy-done.12
  151.0 20.6 %all-to-all-done.5 = f32[8,256,192]{1,2,0:T(8,128)S(1)} async-done(((f32[8,256,192]{1,2,0:T(8,128)}), f32[8,256,192]{1,2,0:T(8,128)S(1)}, u32[]{:S(2)}, u32[]{:S(2)}) %all-to-all-start.5) | async-done | bytes 1572896 | tf_op jit(solution)/shard_map/all_to_all | solution.py:33
  171.6 0.1 reduce_sum.59
  171.7 0.7 fusion.17
  (2 shorter events, 0.0 us)
Async XLA Ops:
  0.0 2.6 %copy-start.1 = (f32[192,1024]{1,0:T(8,128)S(1)}, f32[192,1024]{1,0:T(8,128)}, u32[]{:S(2)}) copy-start(f32[192,1024]{1,0:T(8,128)} %param.18) | copy-start | bytes 2359300
  45.1 1.9 %copy-start.7 = (f32[1024]{0:T(1024)S(1)}, f32[1024]{0:T(1024)}, u32[]{:S(2)}) copy-start(f32[1024]{0:T(1024)} %param.21) | copy-start | bytes 12292
  45.1 2.0 %copy-start.8 = (f32[1024]{0:T(1024)S(1)}, f32[1024]{0:T(1024)}, u32[]{:S(2)}) copy-start(f32[1024]{0:T(1024)} %param.20) | copy-start | bytes 12292
  45.1 14.9 %copy-start.4 = (f32[1024,192]{0,1:T(8,128)S(1)}, f32[1024,192]{0,1:T(8,128)}, u32[]{:S(2)}) copy-start(f32[1024,192]{0,1:T(8,128)} %param.19) | copy-start | bytes 2359300
  60.4 8.5 %copy-start.11 = (f32[192]{0:T(256)S(1)}, f32[192]{0:T(256)}, u32[]{:S(2)}) copy-start(f32[192]{0:T(256)} %param.22) | copy-start | bytes 2308
  61.7 28.6 %copy-start = (bf16[256,192]{0,1:T(8,128)(2,1)S(1)}, bf16[256,192]{0,1:T(8,128)(2,1)}, u32[]{:S(2)}) copy-start(bf16[256,192]{0,1:T(8,128)(2,1)} %param.15) | copy-start | bytes 294916
  61.7 29.6 %copy-start.2 = (f32[192,1024]{1,0:T(8,128)S(1)}, f32[192,1024]{1,0:T(8,128)}, u32[]{:S(2)}) copy-start(f32[192,1024]{1,0:T(8,128)} %param.24) | copy-start | bytes 2359300
  61.7 29.6 %copy-start.6 = (f32[192]{0:T(256)S(1)}, f32[192]{0:T(256)}, u32[]{:S(2)}) copy-start(f32[192]{0:T(256)} %param.23) | copy-start | bytes 2308
  61.7 27.8 %all-to-all-start.2 = ((f32[8,256,192]{1,2,0:T(8,128)}), f32[8,256,192]{1,2,0:T(8,128)S(1)}, u32[]{:S(2)}, u32[]{:S(2)}) async-start(f32[8,256,192]{1,2,0:T(8,128)} %broadcast_in_dim.9), calls=%async_computation.2 | async-start | bytes 3145728 | tf_op jit(solution)/shard_map/all_to_all | solution.py:33
  68.9 22.8 %copy-start.3 = (f32[192,1024]{1,0:T(8,128)S(1)}, f32[192,1024]{1,0:T(8,128)}, u32[]{:S(2)}) copy-start(f32[192,1024]{1,0:T(8,128)} %param.25) | copy-start | bytes 2359300
  128.2 1.9 %copy-start.9 = (f32[1024]{0:T(1024)S(1)}, f32[1024]{0:T(1024)}, u32[]{:S(2)}) copy-start(f32[1024]{0:T(1024)} %param.28) | copy-start | bytes 12292
  128.2 2.0 %copy-start.10 = (f32[1024]{0:T(1024)S(1)}, f32[1024]{0:T(1024)}, u32[]{:S(2)}) copy-start(f32[1024]{0:T(1024)} %param.27) | copy-start | bytes 12292
  128.2 14.8 %copy-start.5 = (f32[1024,192]{0,1:T(8,128)S(1)}, f32[1024,192]{0,1:T(8,128)}, u32[]{:S(2)}) copy-start(f32[1024,192]{0,1:T(8,128)} %param.26) | copy-start | bytes 2359300
  143.3 7.7 %copy-start.12 = (f32[192]{0:T(256)S(1)}, f32[192]{0:T(256)}, u32[]{:S(2)}) copy-start(f32[192]{0:T(256)} %param.29) | copy-start | bytes 2308
  144.6 27.0 %all-to-all-start.5 = ((f32[8,256,192]{1,2,0:T(8,128)}), f32[8,256,192]{1,2,0:T(8,128)S(1)}, u32[]{:S(2)}, u32[]{:S(2)}) async-start(f32[8,256,192]{1,2,0:T(8,128)} %broadcast_in_dim.11), calls=%async_computation.5 | async-start | bytes 3145728 | tf_op jit(solution)/shard_map/all_to_all | solution.py:33
where the time goes:
time: 173 us; the launch traced here: 172 us
  blocking collectives  94.7 us (55%)
  waiting for transfers between devices  41.2 us (24%)
  starting transfers between devices  13.6 us (8%)
  local copies, waits for them, and re-layouts  8.73 us (5%)
  other arithmetic  7.76 us (4%)
  matrix products  6.35 us (4%)
    all_to_all x2, blocking collectives, sum_at_owner(): tiles = lax.all_to_all(split_up(shard, dim, peers), axis, 0, 0, tiled=True)  69.2 us
    all_to_all x2, waiting for transfers between devices, from_everyone(): lax.all_to_all(jnp.broadcast_to(shard[None], (peers, *shard.shape)), axis...  41.2 us
    all_to_all x2, blocking collectives, from_everyone(): lax.all_to_all(jnp.broadcast_to(shard[None], (peers, *shard.shape)), axis...  25.5 us
    all_to_all x2, starting transfers between devices, from_everyone(): lax.all_to_all(jnp.broadcast_to(shard[None], (peers, *shard.shape)), axis...  13.6 us
    concatenate x4, local copies, waits for them, and re-layouts, side_by_side(): both = jnp.concatenate(columns, axis=along)  6 us
    dot_general x2, matrix products, half_step(): jnp.dot(shaped, w_up.astype(jnp.bfloat16), preferred_element_type=jnp.flo...  3.67 us
    reduce_sum x2, other arithmetic, sum_at_owner(): return jnp.sum(tiles, axis=0)  3.64 us
  transfers between devices with their start and end apart: 2, of which 2 were waited for; matrix products, arithmetic and copies ran while one was open for 0% of the time, Pallas kernels for 0%

commit v1 on v0

v1 whole, which is shorter than its diff:
```python
import jax
import jax.numpy as jnp
from jax import lax
from jax.sharding import PartitionSpec as P

D = 3072
PARTS = 1
BF16 = jnp.bfloat16
F32 = jnp.float32


def swap(tiles, axis):
    return lax.all_to_all(tiles, axis, 0, 0, tiled=True)


def to_all(shard, axis):
    peers = lax.axis_size(axis)
    return swap(jnp.broadcast_to(shard[None], (peers, *shard.shape)), axis)


def products(stream, gain, w_gate, w_up):
    squares = jnp.sum(stream * stream, axis=1)
    high = lax.reduce_precision(squares, 8, 7)
    low = squares - high
    shaped = (stream * gain[None, :]).astype(BF16)
    gate = jnp.dot(shaped, w_gate, preferred_element_type=F32).astype(BF16)
    up = jnp.dot(shaped, w_up, preferred_element_type=F32).astype(BF16)
    lane = lax.broadcasted_iota(jnp.int32, (stream.shape[0], 128), 1)
    extra = jnp.where(lane == 0, high[:, None], jnp.where(lane == 1, low[:, None], 0.0)).astype(BF16)
    both = jnp.concatenate([gate, up, extra], axis=1)
    peers = lax.axis_size("ra")
    return both.reshape(peers, -1, both.shape[1])


def hidden_of(tiles, gate_scale, up_scale):
    total = jnp.sum(tiles.astype(F32), axis=0)
    units = gate_scale.shape[0]
    squares = total[:, 2 * units] + total[:, 2 * units + 1]
    inverse = lax.rsqrt(squares / D + 1e-06)[:, None]
    gate = inverse * gate_scale[None, :] * total[:, :units]
    up = inverse * up_scale[None, :] * total[:, units : 2 * units]
    return (jax.nn.silu(gate) * up).astype(BF16)


def half_step(streams, gain, w_gate, w_up, w_down, gate_scale, up_scale, down_scale):
    w_gate, w_up, w_down = (w.astype(BF16) for w in (w_gate, w_up, w_down))
    scale = 0.5 * down_scale
    results = []
    for stream_in in streams:
        stream = stream_in.astype(F32)
        tiles = swap(products(stream, gain, w_gate, w_up), "ra")
        hidden = to_all(hidden_of(tiles, gate_scale, up_scale), "ra")
        hidden = hidden.reshape(-1, hidden.shape[-1])
        down = jnp.dot(hidden, w_down, preferred_element_type=F32).astype(BF16)
        total = jnp.sum(to_all(down, "cb").astype(F32), axis=0)
        results.append((stream + scale[None, :] * total).astype(BF16))
    return results


def body(tokens, *rest):
    streams = jnp.split(tokens, PARTS, axis=0)
    streams = half_step(streams, *rest[:7])
    streams = half_step(streams, *rest[7:])
    return jnp.concatenate(streams, axis=0)


def solution(mesh):
    one = (P("ra"), P("ra", "cb"), P("ra", "cb"), P("cb", "ra"), P("cb"), P("cb"), P("ra"))
    return jax.shard_map(
        body, mesh=mesh, in_specs=(P(None, "ra"), *one, *one), out_specs=P(None, "ra"), check_vma=False
    )
```

time: 173 us -> 119 us (0.69)
  blocking collectives: 94.7 us -> 69.3 us
  waiting for transfers between devices: 41.2 us -> 24.3 us
  local copies, waits for them, and re-layouts: 8.73 us -> 3.29 us
  other arithmetic: 7.76 us -> 3.41 us
  matrix products: 6.35 us -> 3.43 us
    all_to_all x4, blocking collectives: 94.7 us -> 69.3 us  [swap(): return lax.all_to_all(tiles, axis, 0, 0, tiled=True)]
    all_to_all x2, waiting for transfers between devices: 41.2 us -> 24.3 us  [swap(): return lax.all_to_all(tiles, axis, 0, 0, tiled=True)]
    concatenate x4 -> x0, local copies, waits for them, and re-layouts: 6 us -> none  [side_by_side(): both = jnp.concatenate(columns, axis=along)]
    reduce_sum x6, other arithmetic: 6.57 us -> 1.63 us  [the longest x2 1.13 us: products(): squares = jnp.sum(stream * stream, axis=1)]
    dot_general x6, matrix products: 6.35 us -> 3.43 us  [the longest x2 1.99 us: products(): up = jnp.dot(shaped, w_up, preferred_element_type=F32).astype(BF16)]
where the time goes in v1:
time: 119 us; the launch traced here: 118 us
  blocking collectives  69.3 us (58%)
  waiting for transfers between devices  24.3 us (20%)
  starting transfers between devices  14.1 us (12%)
  matrix products  3.43 us (3%)
  other arithmetic  3.41 us (3%)
  local copies, waits for them, and re-layouts  3.29 us (3%)
    all_to_all x4, blocking collectives, swap(): return lax.all_to_all(tiles, axis, 0, 0, tiled=True)  69.3 us
    all_to_all x2, waiting for transfers between devices, swap(): return lax.all_to_all(tiles, axis, 0, 0, tiled=True)  24.3 us
    all_to_all x2, starting transfers between devices, swap(): return lax.all_to_all(tiles, axis, 0, 0, tiled=True)  14.1 us
  transfers between devices with their start and end apart: 2, of which 2 were waited for; matrix products, arithmetic and copies ran while one was open for 0% of the time, Pallas kernels for 0%

profile of v1, /device:TPU:1, one launch (start us, length us, event | category | flops | bytes accessed | tf_op | source)
XLA Modules:
  0.0 118.0 jit_solution(13328891134768420492)
XLA Ops:
  0.0 0.0 copy-start
  0.0 0.0 copy-start.6
  0.0 0.0 copy-start.1
  0.0 1.0 fusion.7
  1.0 1.6 %convolution_convert_fusion.2 = bf16[256,1024]{1,0:T(8,128)(2,1)S(1)} fusion(f32[192,1024]{1,0:T(8,128)} %param.18, bf16[256,192]{0,1:T(8,128)(2,1)} %param.15, f32[192]{0:T(256)} %param.16), kind=kOutput, calls=%fused_computation.6 | convolution fusion | flops 101269504 | bytes 1409792 | tf_op jit(solution)/shard_map/dot_general | solution.py:27
  2.6 0.0 copy-done
  2.7 0.0 copy-done.6
  2.7 0.0 copy-done.1
  2.7 0.4 convolution_convert_fusion.3
  3.1 0.1 select_convert_fusion.1
  3.2 0.1 pad_maximum_fusion
  3.3 25.3 %all_to_all.30 = bf16[16,16,2176]{2,1,0:T(8,128)(2,1)S(1)} all-to-all(bf16[16,16,2176]{2,1,0:T(8,128)(2,1)S(1)} %bitcast.6), channel_id=1, replica_groups=mesh['ra'=16,'cb'=8] {'ra'}, dimensions={0} | all-to-all | bytes 2228224 | tf_op jit(solution)/shard_map/all_to_all | solution.py:13
  28.6 0.0 copy-start.8
  28.6 0.0 copy-start.9
  28.6 0.2 convert_reduce_fusion.1
  28.8 0.0 copy-start.4
  28.8 0.2 fusion.27
  29.0 0.3 copy-done.8
  29.3 0.0 copy-done.9
  29.3 0.1 fusion.15
  29.4 0.1 broadcast_in_dim.42
  29.5 12.5 %all_to_all.31 = bf16[16,16,1024]{2,1,0:T(8,128)(2,1)S(1)} all-to-all(bf16[16,16,1024]{2,1,0:T(8,128)(2,1)S(1)} %broadcast_in_dim.42), channel_id=1, replica_groups=mesh['ra'=16,'cb'=8] {'ra'}, dimensions={0} | all-to-all | bytes 1048576 | tf_op jit(solution)/shard_map/all_to_all | solution.py:13
  42.0 0.0 copy-done.4
  42.0 0.3 convolution_convert_fusion.5
  42.3 0.0 copy-start.12
  42.3 0.9 broadcast_in_dim.43
  43.2 0.0 copy-start.2
  43.2 0.0 copy-start.7
  43.2 7.4 %all-to-all-start.2 = ((bf16[8,256,192]{1,2,0:T(8,128)(2,1)}), bf16[8,256,192]{1,2,0:T(8,128)(2,1)S(1)}, u32[]{:S(2)}, u32[]{:S(2)}) async-start(bf16[8,256,192]{1,2,0:T(8,128)(2,1)} %broadcast_in_dim.43), calls=%async_computation.2 | async-start | bytes 1572864 | tf_op jit(solution)/shard_map/all_to_all | solution.py:13
  50.7 0.0 copy-done.12
  50.7 12.2 %all-to-all-done.2 = bf16[8,256,192]{1,2,0:T(8,128)(2,1)S(1)} async-done(((bf16[8,256,192]{1,2,0:T(8,128)(2,1)}), bf16[8,256,192]{1,2,0:T(8,128)(2,1)S(1)}, u32[]{:S(2)}, u32[]{:S(2)}) %all-to-all-start.2) | async-done | bytes 786464 | tf_op jit(solution)/shard_map/all_to_all | solution.py:13
  62.8 0.1 convert_reduce_fusion.3
  62.9 0.0 copy-start.3
  62.9 0.1 fusion.10
  63.1 0.0 copy-done.2
  63.1 0.0 copy-done.7
  63.1 0.4 convolution_convert_fusion
  63.5 0.6 copy-done.3
  64.1 0.4 convolution_convert_fusion.1
  64.5 0.1 select_convert_fusion
  64.6 0.1 pad_maximum_fusion.1
  64.7 19.3 %all_to_all.32 = bf16[16,16,2176]{2,1,0:T(8,128)(2,1)S(1)} all-to-all(bf16[16,16,2176]{2,1,0:T(8,128)(2,1)S(1)} %bitcast.7), channel_id=1, replica_groups=mesh['ra'=16,'cb'=8] {'ra'}, dimensions={0} | all-to-all | bytes 2228224 | tf_op jit(solution)/shard_map/all_to_all | solution.py:13
  84.0 0.0 copy-start.10
  84.0 0.0 copy-start.11
  84.0 0.2 convert_reduce_fusion
  84.2 0.0 copy-start.5
  84.2 0.2 fusion.23
  84.4 0.3 copy-done.10
  84.7 0.0 copy-done.11
  84.7 0.1 fusion.13
  84.8 0.1 broadcast_in_dim.76
  84.9 12.2 %all_to_all.33 = bf16[16,16,1024]{2,1,0:T(8,128)(2,1)S(1)} all-to-all(bf16[16,16,1024]{2,1,0:T(8,128)(2,1)S(1)} %broadcast_in_dim.76), channel_id=1, replica_groups=mesh['ra'=16,'cb'=8] {'ra'}, dimensions={0} | all-to-all | bytes 1048576 | tf_op jit(solution)/shard_map/all_to_all | solution.py:13
  97.0 0.0 copy-done.5
  97.0 0.3 convolution_convert_fusion.4
  97.4 0.0 copy-start.13
  97.4 0.9 broadcast_in_dim.77
  98.3 6.6 %all-to-all-start.5 = ((bf16[8,256,192]{1,2,0:T(8,128)(2,1)}), bf16[8,256,192]{1,2,0:T(8,128)(2,1)S(1)}, u32[]{:S(2)}, u32[]{:S(2)}) async-start(bf16[8,256,192]{1,2,0:T(8,128)(2,1)} %broadcast_in_dim.77), calls=%async_computation.5 | async-start | bytes 1572864 | tf_op jit(solution)/shard_map/all_to_all | solution.py:13
  105.0 0.0 copy-done.13
  105.0 12.2 %all-to-all-done.5 = bf16[8,256,192]{1,2,0:T(8,128)(2,1)S(1)} async-done(((bf16[8,256,192]{1,2,0:T(8,128)(2,1)}), bf16[8,256,192]{1,2,0:T(8,128)(2,1)S(1)}, u32[]{:S(2)}, u32[]{:S(2)}) %all-to-all-start.5) | async-done | bytes 786464 | tf_op jit(solution)/shard_map/all_to_all | solution.py:13
  117.2 0.1 convert_reduce_fusion.2
  117.3 0.7 fusion.11
  (5 shorter events, 0.0 us)
Async XLA Ops:
  0.0 2.7 %copy-start = (bf16[256,192]{0,1:T(8,128)(2,1)S(1)}, bf16[256,192]{0,1:T(8,128)(2,1)}, u32[]{:S(2)}) copy-start(bf16[256,192]{0,1:T(8,128)(2,1)} %param.15) | copy-start | bytes 294916
  0.0 2.7 %copy-start.6 = (f32[192]{0:T(256)S(1)}, f32[192]{0:T(256)}, u32[]{:S(2)}) copy-start(f32[192]{0:T(256)} %param.16) | copy-start | bytes 2308
  0.0 2.7 %copy-start.1 = (f32[192,1024]{1,0:T(8,128)S(1)}, f32[192,1024]{1,0:T(8,128)}, u32[]{:S(2)}) copy-start(f32[192,1024]{1,0:T(8,128)} %param.17) | copy-start | bytes 2359300
  28.6 0.7 copy-start.8
  28.6 0.7 copy-start.9
  28.8 13.2 %copy-start.4 = (f32[1024,192]{0,1:T(8,128)S(1)}, f32[1024,192]{0,1:T(8,128)}, u32[]{:S(2)}) copy-start(f32[1024,192]{0,1:T(8,128)} %param.19) | copy-start | bytes 2359300
  42.3 8.4 %copy-start.12 = (f32[192]{0:T(256)S(1)}, f32[192]{0:T(256)}, u32[]{:S(2)}) copy-start(f32[192]{0:T(256)} %param.22) | copy-start | bytes 2308
  43.2 19.8 %copy-start.2 = (f32[192,1024]{1,0:T(8,128)S(1)}, f32[192,1024]{1,0:T(8,128)}, u32[]{:S(2)}) copy-start(f32[192,1024]{1,0:T(8,128)} %param.25) | copy-start | bytes 2359300
  43.2 19.8 %copy-start.7 = (f32[192]{0:T(256)S(1)}, f32[192]{0:T(256)}, u32[]{:S(2)}) copy-start(f32[192]{0:T(256)} %param.23) | copy-start | bytes 2308
  43.2 19.6 %all-to-all-start.2 = ((bf16[8,256,192]{1,2,0:T(8,128)(2,1)}), bf16[8,256,192]{1,2,0:T(8,128)(2,1)S(1)}, u32[]{:S(2)}, u32[]{:S(2)}) async-start(bf16[8,256,192]{1,2,0:T(8,128)(2,1)} %broadcast_in_dim.43), calls=%async_computation.2 | async-start | bytes 1572864 | tf_op jit(solution)/shard_map/all_to_all | solution.py:13
  62.9 1.1 copy-start.3
  84.0 0.7 copy-start.10
  84.0 0.7 copy-start.11
  84.2 12.9 %copy-start.5 = (f32[1024,192]{0,1:T(8,128)S(1)}, f32[1024,192]{0,1:T(8,128)}, u32[]{:S(2)}) copy-start(f32[1024,192]{0,1:T(8,128)} %param.26) | copy-start | bytes 2359300
  97.4 7.6 %copy-start.13 = (f32[192]{0:T(256)S(1)}, f32[192]{0:T(256)}, u32[]{:S(2)}) copy-start(f32[192]{0:T(256)} %param.29) | copy-start | bytes 2308
  98.3 18.8 %all-to-all-start.5 = ((bf16[8,256,192]{1,2,0:T(8,128)(2,1)}), bf16[8,256,192]{1,2,0:T(8,128)(2,1)S(1)}, u32[]{:S(2)}, u32[]{:S(2)}) async-start(bf16[8,256,192]{1,2,0:T(8,128)(2,1)} %broadcast_in_dim.77), calls=%async_computation.5 | async-start | bytes 1572864 | tf_op jit(solution)/shard_map/all_to_all | solution.py:13
